TPU v7x, 32 devices: a whole 2x2x4 slice. The times are simulated.
32 devices in a mesh: ep: 16 (over z, y, core), tp: 2 (over x).
Axes of the slice: x: 2, y: 2, z: 4, core: 2. Of those that a mesh axis runs over, the one named last changes fastest.
Arguments:
- tokens: bfloat16 [256, 2048], P('ep'), may hold values from -6 to 6
- positions: int32 [256], P('ep'), may hold values from 1024 to 16383
- state: float32 [256, 4, 128, 128], P('ep', 'tp'), may hold values from -1 to 1
- mix_gain: float32 [2048], replicated, may hold values from 0.1 to 1.9
- w_query: bfloat16 [2048, 512], P(None, 'tp'), may hold values from -0.125 to 0.125
- w_key: bfloat16 [2048, 512], P(None, 'tp'), may hold values from -0.125 to 0.125
- w_value: bfloat16 [2048, 512], P(None, 'tp'), may hold values from -0.125 to 0.125
- w_out: bfloat16 [512, 2048], P('tp'), may hold values from -0.25 to 0.25
- ffn_gain: float32 [2048], replicated, may hold values from 0.1 to 1.9
- branch_gate: bfloat16 [2048], replicated, may hold values from -0.125 to 0.125
- dense_gate: bfloat16 [2048, 4096], P('tp', 'ep'), may hold values from -0.125 to 0.125
- dense_up: bfloat16 [2048, 4096], P('tp', 'ep'), may hold values from -0.125 to 0.125
- dense_down: bfloat16 [4096, 2048], P('ep', 'tp'), may hold values from -0.09375 to 0.09375
- routes: int32 [256, 6], P('ep'), may hold values from 0 to 15, all different within a row; in each aligned block of 16 rows (0 to 15, 16 to 31, ...) at most 12 rows name the same one
- route_scores: float32 [256, 6], P('ep'), may hold values from 0.05 to 1
- expert_gate: bfloat16 [16, 2048, 512], P('ep', None, 'tp'), may hold values from -0.125 to 0.125
- expert_up: bfloat16 [16, 2048, 512], P('ep', None, 'tp'), may hold values from -0.125 to 0.125
- expert_down: bfloat16 [16, 512, 2048], P('ep', 'tp'), may hold values from -0.25 to 0.25
Outputs:
- layer_out: bfloat16 [256, 2048], P('ep', 'tp')
Inputs may be any that keep to these rules, and one draw needn't show every extreme that they name: `routes`: each row names 6 different experts. In each aligned block of 16 rows (the rows of one index of ep) no expert is named by more than 12 rows, a bound that some block reaches.
All inputs are finite; a program needn't handle non-finite values.
Results may differ from a plain program's by a relative error of at most 0.012.
Values may be sent and summed in bfloat16 or wider, within the bound.
A program may use at most 64 MiB of HBM per device.

v0:
```python
import jax
import jax.numpy as jnp
from jax import lax
from jax.sharding import PartitionSpec as P

EPS = 1e-06


def normalize(inputs, scale_vec):
    values = inputs.astype(jnp.float32)
    return values * lax.rsqrt(jnp.mean(values * values, axis=-1, keepdims=True) + EPS) * scale_vec


def rotate(vectors, where):
    half = vectors.shape[-1] // 2
    inverse = 1.0 / 10000.0 ** jnp.linspace(0.0, 1.0, half, dtype=jnp.float32)
    angle = where.astype(jnp.float32)[:, None] * inverse[None, :]
    cosine = jnp.cos(angle)[:, None, :]
    sine = jnp.sin(angle)[:, None, :]
    first = vectors[..., :half]
    second = vectors[..., half:]
    return jnp.concatenate(
        [first * cosine - second * sine, second * cosine + first * sine], axis=-1
    )


def on_device(
    tokens,
    positions,
    state,
    mix_gain,
    w_query,
    w_key,
    w_value,
    w_out,
    ffn_gain,
    branch_gate,
    dense_gate,
    dense_up,
    dense_down,
    routes,
    route_scores,
    expert_gate,
    expert_up,
    expert_down,
):
    sequences = tokens.shape[0]
    model_width = tokens.shape[1]
    tp_count = lax.axis_size("tp")
    ep_count = lax.axis_size("ep")
    columns = model_width // tp_count
    tp_index = lax.axis_index("tp")
    local_heads = state.shape[1]
    head_dim = state.shape[2]
    normed = normalize(tokens, mix_gain).astype(jnp.bfloat16)
    query_vec = jnp.dot(normed, w_query, preferred_element_type=jnp.float32).reshape(
        sequences, local_heads, head_dim
    )
    key_vec = jnp.dot(normed, w_key, preferred_element_type=jnp.float32).reshape(
        sequences, local_heads, head_dim
    )
    value_vec = jnp.dot(normed, w_value, preferred_element_type=jnp.float32).reshape(
        sequences, local_heads, head_dim
    )
    query_vec = rotate(query_vec, positions)
    key_vec = rotate(key_vec, positions) * head_dim ** (-0.5)
    all_heads = local_heads * tp_count
    head_index = (tp_index * local_heads + jnp.arange(local_heads, dtype=jnp.int32)).astype(
        jnp.float32
    )
    decay_rate = 1.0 - 2.0 ** (-5.0 - 5.0 * head_index / (all_heads - 1))
    new_state = (
        decay_rate[None, :, None, None] * state + key_vec[:, :, :, None] * value_vec[:, :, None, :]
    )
    retrieved = jnp.einsum("bhd,bhde->bhe", query_vec, new_state, precision=lax.Precision.HIGHEST)
    retrieved = retrieved * lax.rsqrt(jnp.mean(retrieved * retrieved, axis=-1, keepdims=True) + EPS)
    retrieved = retrieved.reshape(sequences, local_heads * head_dim).astype(jnp.bfloat16)
    head_partial = jnp.dot(retrieved, w_out, preferred_element_type=jnp.float32).astype(
        jnp.bfloat16
    )
    mixer_out = lax.psum(head_partial.astype(jnp.float32).astype(jnp.bfloat16), "tp").astype(
        jnp.float32
    )
    after_mix = tokens.astype(jnp.float32) + mixer_out
    ffn_in = normalize(after_mix, ffn_gain).astype(jnp.bfloat16)
    own_cols = lax.dynamic_slice_in_dim(ffn_in, tp_index * columns, columns, 1)
    per_device = expert_gate.shape[0]
    experts = per_device * ep_count
    fanout = routes.shape[1]
    capacity = max(2, min(sequences, 2 * sequences * fanout // experts))
    slot_count = experts * capacity
    marks = (routes[:, :, None] == jnp.arange(experts, dtype=jnp.int32)[None, None, :]).astype(
        jnp.int32
    )
    flattened = marks.reshape(sequences * fanout, experts)
    ranking = jnp.sum((jnp.cumsum(flattened, axis=0) - flattened) * flattened, axis=1).reshape(
        sequences, fanout
    )
    slot_index = routes * capacity + ranking
    matches = jnp.arange(slot_count, dtype=jnp.int32)[:, None, None] == slot_index[None]
    placing = jnp.any(matches, axis=2).astype(jnp.bfloat16)
    route_weights = route_scores / jnp.sum(route_scores, axis=1, keepdims=True)
    combining = jnp.sum(jnp.where(matches, route_weights[None], 0.0), axis=2).T
    packed = jnp.dot(placing, own_cols, preferred_element_type=jnp.float32).astype(jnp.bfloat16)
    packed = packed.reshape(experts, capacity, own_cols.shape[1])
    received = lax.all_to_all(packed, "ep", split_axis=0, concat_axis=0, tiled=True)
    received = lax.all_gather(received, "tp", axis=2, tiled=True)
    count = received.shape[1]
    grouped = received.reshape(ep_count, per_device, count, model_width)
    gate_pre = jnp.einsum(
        "skcd,kdw->skcw", grouped, expert_gate, preferred_element_type=jnp.float32
    )
    up_pre = jnp.einsum("skcd,kdw->skcw", grouped, expert_up, preferred_element_type=jnp.float32)
    hidden = (jax.nn.silu(gate_pre) * up_pre).astype(jnp.bfloat16)
    partial_out = jnp.einsum(
        "skcw,kwd->skcd", hidden, expert_down, preferred_element_type=jnp.float32
    )
    blocks_out = partial_out.astype(jnp.bfloat16).reshape(
        ep_count, per_device, count, tp_count, columns
    )
    traded = lax.all_to_all(blocks_out, "tp", split_axis=3, concat_axis=3, tiled=True)
    mine = jnp.sum(traded.astype(jnp.float32), axis=3).astype(jnp.bfloat16)
    mine = mine.reshape(ep_count * per_device, count, columns)
    returned = lax.all_to_all(mine, "ep", split_axis=0, concat_axis=0, tiled=True)
    experts_out = jnp.dot(
        combining,
        returned.reshape(slot_count, columns).astype(jnp.float32),
        precision=lax.Precision.HIGHEST,
    )
    hidden_units = dense_gate.shape[1]
    both_weights = jnp.concatenate([dense_gate, dense_up], axis=1)
    pre_parts = jnp.dot(
        lax.all_gather(own_cols, "ep", axis=0, tiled=True),
        both_weights,
        preferred_element_type=jnp.float32,
    ).astype(jnp.bfloat16)
    pre_total = lax.psum(pre_parts.astype(jnp.float32).astype(jnp.bfloat16), "tp").astype(
        jnp.float32
    )
    dense_hidden = (jax.nn.silu(pre_total[:, :hidden_units]) * pre_total[:, hidden_units:]).astype(
        jnp.bfloat16
    )
    dense_out = lax.psum_scatter(
        jnp.dot(dense_hidden, dense_down, preferred_element_type=jnp.float32),
        "ep",
        scatter_dimension=0,
        tiled=True,
    )
    branch_weight = jax.nn.sigmoid(jnp.dot(ffn_in, branch_gate, preferred_element_type=jnp.float32))
    residual_cols = lax.dynamic_slice_in_dim(after_mix, tp_index * columns, columns, 1)
    layer_out = residual_cols + experts_out + branch_weight[:, None] * dense_out
    return layer_out.astype(jnp.bfloat16)


def solution(mesh):
    placed = (
        P("ep", None),
        P("ep"),
        P("ep", "tp", None, None),
        P(),
        P(None, "tp"),
        P(None, "tp"),
        P(None, "tp"),
        P("tp", None),
        P(),
        P(),
        P("tp", "ep"),
        P("tp", "ep"),
        P("ep", "tp"),
        P("ep", None),
        P("ep", None),
        P("ep", None, "tp"),
        P("ep", None, "tp"),
        P("ep", "tp", None),
    )
    return jax.shard_map(
        on_device, mesh=mesh, in_specs=placed, out_specs=P("ep", "tp"), check_vma=False
    )
```

profile of v0, /device:TPU:0, one launch (start us, length us, event | category | flops | bytes accessed | tf_op | source)
XLA Modules:
  0.0 169.2 jit_solution(17816289287856958037)
XLA Ops:
  6.5 0.0 copy-start
  6.5 0.0 all-reduce.3.cloned.1.call-start
  6.6 0.8 convert_element_type.77
  7.4 1.0 fusion.30
  8.5 1.6 fusion.47
  10.1 1.6 fusion.45
  11.6 0.0 copy-done.1
  11.7 0.0 copy-done.7
  11.7 1.5 fusion.49
  13.2 0.0 copy-start.3
  13.2 0.1 fusion.41
  13.3 0.1 multiply_cosine_fusion
  13.4 0.0 copy-start.10
  13.4 0.1 multiply_subtract_fusion
  13.5 0.1 pad_maximum_fusion
  13.7 2.1 %fusion = f32[16,2,1,128]{3,2,1,0:T(1,128)S(1)} fusion(f32[16,2,128,1]{2,3,1,0:T(1,128)S(1)} %bitcast.86, f32[16,2,128,128]{3,2,1,0:T(8,128)S(1)} %copy-done.2, f32[16,2,128]{2,1,0:T(2,128)S(1)} %mul.244, f32[16,2,128]{2,1,0:T(2,128)S(1)} %get-tuple-element.17, f32[2]{0:T(128)S(1)} %power_subtract_fusion), kind=kOutput, calls=%fused_computation.2 | convolution fusion | flops 7864320 | bytes 2162696 | tf_op jit(solution)/shard_map/bhd,bhde->bhe/dot_general | solution.py:75
  15.7 0.1 multiply_reduce_fusion.1
  15.8 0.1 multiply_convert_fusion.1
  15.9 0.0 copy-done.3
  15.9 0.9 convolution_convert_fusion.1
  16.8 0.0 all-reduce.3.cloned.1.call-update
  16.9 0.1 copy.59
  16.9 0.1 eq.30
  17.0 0.1 fusion.38
  17.1 0.1 reduce_window_sum.11
  17.3 0.2 select_reduce_fusion.1
  17.4 0.1 reshape.154
  17.5 0.1 copy.60
  17.6 0.1 fusion.37
  17.7 23.0 %all-reduce.3.cloned.1.call-done = bf16[16,2048]{1,0:T(8,128)(2,1)} async-done(((bf16[16,2048]{1,0:T(8,128)(2,1)}), bf16[16,2048]{1,0:T(8,128)(2,1)}) %all-reduce.3.cloned.1.call-update) | async-done | bytes 65552 | tf_op jit(solution)/shard_map/psum | solution.py:81
  40.7 1.6 convert_add_fusion
  42.3 0.9 multiply_convert_fusion
  43.3 22.9 %all_gather.7 = bf16[256,1024]{1,0:T(8,128)(2,1)S(1)} all-gather(bf16[16,1024]{1,0:T(8,128)(2,1)S(1)} %constant_dynamic-slice_fusion), channel_id=1, replica_groups=mesh['ep'=16,'tp'=2] {'ep'}, dimensions={0}, use_global_device_ids=true | all-gather | bytes 557056 | tf_op jit(solution)/shard_map/all_gather | solution.py:133
  66.2 0.3 convolution_convert_fusion.2
  66.5 0.9 reshape.155
  67.4 3.6 %all-to-all-start = ((bf16[16,12,1024]{2,1,0:T(8,128)(2,1)}), bf16[16,12,1024]{2,1,0:T(8,128)(2,1)S(1)}, u32[]{:S(2)}, u32[]{:S(2)}) async-start(bf16[16,12,1024]{2,1,0:T(8,128)(2,1)} %reshape.155), calls=%async_computation | async-start | bytes 1048576 | tf_op jit(solution)/shard_map/all_to_all | solution.py:106
  70.9 0.0 copy-start.5
  71.0 0.0 all-reduce.5.cloned.1.call-start
  71.0 2.2 %convolution_convert_fusion.3 = bf16[256,512]{1,0:T(8,128)(2,1)} fusion(bf16[256,1024]{1,0:T(8,128)(2,1)S(1)} %all_gather.7, bf16[1024,256]{1,0:T(8,128)(2,1)S(1)} %copy-done.12, bf16[1024,256]{1,0:T(8,128)(2,1)} %param.30), kind=kOutput, calls=%fused_computation.7 | convolution fusion | flops 270663680 | bytes 1835008 | tf_op jit(solution)/shard_map/dot_general | solution.py:132
  73.2 0.0 all-reduce.5.cloned.1.call-update
  73.3 0.0 reduce-scatter.2.cloned.1.call-start
  73.3 24.4 %all-reduce.5.cloned.1.call-done = bf16[256,512]{1,0:T(8,128)(2,1)} async-done(((bf16[256,512]{1,0:T(8,128)(2,1)}), bf16[256,512]{1,0:T(8,128)(2,1)}) %all-reduce.5.cloned.1.call-update) | async-done | bytes 262160 | tf_op jit(solution)/shard_map/psum | solution.py:137
  97.7 1.0 convert_element_type.92
  98.8 0.0 copy-start.4
  98.8 1.3 fusion.33
  100.1 0.0 reduce-scatter.2.cloned.1.call-update
  100.1 0.0 all-to-all-done
  100.1 0.2 copy.61
  100.3 11.0 %all_gather.6 = bf16[16,12,2048]{2,0,1:T(8,128)(2,1)S(1)} all-gather(bf16[16,12,1024]{2,0,1:T(8,128)(2,1)S(1)} %copy.61), channel_id=1, replica_groups=mesh['ep'=16,'tp'=2] {'tp'}, dimensions={2}, use_global_device_ids=true | all-gather | bytes 1179648 | tf_op jit(solution)/shard_map/all_gather | solution.py:107
  111.4 1.1 convolution_bitcast_fusion.1
  112.4 2.3 %convolution_convert_fusion = bf16[16,12,2048]{2,0,1:T(8,128)(2,1)S(1)} fusion(bf16[1,256,2048]{2,1,0:T(8,128)(2,1)S(1)} %copy-done, bf16[16,12,2048]{2,0,1:T(8,128)(2,1)S(1)} %all_gather.6, bf16[1,2048,256]{2,1,0:T(8,128)(2,1)} %param.36, f32[16,1,12,256]{3,0,2,1:T(8,128)} %convolution_bitcast_fusion.1), kind=kOutput, calls=%fused_computation | convolution fusion | flops 403341312 | bytes 3866624 | tf_op jit(solution)/shard_map/skcw,kwd->skcd/dot_general | solution.py:115
  114.7 0.1 copy.77
  114.8 0.0 copy-start.11
  114.8 0.0 copy-start.9
  114.8 12.1 %all_to_all.15 = bf16[16,1,12,2,1024]{4,0,2,1,3:T(8,128)(2,1)S(1)} all-to-all(bf16[16,1,12,2,1024]{4,0,2,1,3:T(8,128)(2,1)S(1)} %bitcast.82), channel_id=1, replica_groups=mesh['ep'=16,'tp'=2] {'tp'}, dimensions={3} | all-to-all | bytes 1572864 | tf_op jit(solution)/shard_map/all_to_all | solution.py:121
  126.9 0.2 reduce_sum.72
  127.1 1.0 copy.64
  128.2 5.6 %all-to-all-start.2 = ((bf16[16,12,1024]{2,1,0:T(8,128)(2,1)}), bf16[16,12,1024]{2,1,0:T(8,128)(2,1)S(1)}, u32[]{:S(2)}, u32[]{:S(2)}) async-start(bf16[16,12,1024]{2,1,0:T(8,128)(2,1)} %copy.64), calls=%async_computation.2 | async-start | bytes 1048576 | tf_op jit(solution)/shard_map/all_to_all | solution.py:124
  133.9 0.1 select_reduce_fusion
  134.0 0.1 fusion.12
  134.1 14.8 %all-to-all-done.2 = bf16[16,12,1024]{2,1,0:T(8,128)(2,1)S(1)} async-done(((bf16[16,12,1024]{2,1,0:T(8,128)(2,1)}), bf16[16,12,1024]{2,1,0:T(8,128)(2,1)S(1)}, u32[]{:S(2)}, u32[]{:S(2)}) %all-to-all-start.2) | async-done | bytes 393248 | tf_op jit(solution)/shard_map/all_to_all | solution.py:124
  148.9 0.1 reshape.161
  149.0 11.9 %reduce-scatter.2.cloned.1.call-done = f32[16,1024]{1,0:T(8,128)} async-done(((f32[256,1024]{1,0:T(8,128)}), f32[16,1024]{1,0:T(8,128)}) %reduce-scatter.2.cloned.1.call-update) | async-done | bytes 65552 | tf_op jit(solution)/shard_map/reduce_scatter | solution.py:143
  160.9 1.7 %fusion.8 = bf16[16,1024]{1,0:T(8,128)(2,1)} fusion(f32[192,16]{0,1:T(8,128)S(1)} %select_reduce_fusion, bf16[192,1024]{1,0:T(8,128)(2,1)S(1)} %reshape.161, f32[16,1024]{1,0:T(8,128)} %reduce-scatter.2.cloned.1.call-done, f32[16,2048]{1,0:T(8,128)S(1)} %copy-done.6, s32[]{:T(128)S(6)} %select_n.8, f32[16]{0:T(128)S(1)} %fusion.12), kind=kOutput, calls=%fused_computation.15 | convolution fusion | flops 37814272 | bytes 569412 | tf_op jit(solution)/shard_map/dot_general | solution.py:125
  (29 shorter events, 0.2 us)
Async XLA Ops:
  6.5 105.9 %copy-start = (bf16[1,256,2048]{2,1,0:T(8,128)(2,1)S(1)}, bf16[1,256,2048]{2,1,0:T(8,128)(2,1)}, u32[]{:S(2)}) copy-start(bf16[1,256,2048]{2,1,0:T(8,128)(2,1)} %param.37) | copy-start | bytes 3145732
  6.5 5.1 %copy-start.1 = (bf16[16,2048]{1,0:T(8,128)(2,1)S(1)}, bf16[16,2048]{1,0:T(8,128)(2,1)}, u32[]{:S(2)}) copy-start(bf16[16,2048]{1,0:T(8,128)(2,1)} %param.20) | copy-start | bytes 196612
  6.5 5.1 %copy-start.7 = (f32[2048]{0:T(1024)S(1)}, f32[2048]{0:T(1024)}, u32[]{:S(2)}) copy-start(f32[2048]{0:T(1024)} %param.23) | copy-start | bytes 24580
  6.5 7.1 %copy-start.2 = (f32[16,2,128,128]{3,2,1,0:T(8,128)S(1)}, f32[16,2,128,128]{3,2,1,0:T(8,128)}, u32[]{:S(2)}) copy-start(f32[16,2,128,128]{3,2,1,0:T(8,128)} %param.22) | copy-start | bytes 6291460
  6.5 34.1 %all-reduce.3.cloned.1.call-start = ((), (), s32[]{:S(2)}) async-start(), calls=%async_computation.4 | async-start | bytes 131072 | tf_op jit(solution)/shard_map/psum | solution.py:81
  13.2 3.7 %copy-start.8 = (s32[16,6]{0,1:T(8,128)S(1)}, s32[16,6]{0,1:T(8,128)}, u32[]{:S(2)}) copy-start(s32[16,6]{0,1:T(8,128)} %param.33) | copy-start | bytes 1156
  13.2 2.7 %copy-start.3 = (bf16[256,2048]{1,0:T(8,128)(2,1)S(1)}, bf16[256,2048]{1,0:T(8,128)(2,1)}, u32[]{:S(2)}) copy-start(bf16[256,2048]{1,0:T(8,128)(2,1)} %param.27) | copy-start | bytes 3145732
  13.4 28.9 %copy-start.10 = (f32[2048]{0:T(1024)S(1)}, f32[2048]{0:T(1024)}, u32[]{:S(2)}) copy-start(f32[2048]{0:T(1024)} %param.28) | copy-start | bytes 24580
  16.8 54.2 %copy-start.12 = (bf16[1024,256]{1,0:T(8,128)(2,1)S(1)}, bf16[1024,256]{1,0:T(8,128)(2,1)}, u32[]{:S(2)}) copy-start(bf16[1024,256]{1,0:T(8,128)(2,1)} %param.31) | copy-start | bytes 1572868
  67.4 32.7 %all-to-all-start = ((bf16[16,12,1024]{2,1,0:T(8,128)(2,1)}), bf16[16,12,1024]{2,1,0:T(8,128)(2,1)S(1)}, u32[]{:S(2)}, u32[]{:S(2)}) async-start(bf16[16,12,1024]{2,1,0:T(8,128)(2,1)} %reshape.155), calls=%async_computation | async-start | bytes 1048576 | tf_op jit(solution)/shard_map/all_to_all | solution.py:106
  70.9 27.8 %copy-start.5 = (bf16[256,1024]{1,0:T(8,128)(2,1)S(1)}, bf16[256,1024]{1,0:T(8,128)(2,1)}, u32[]{:S(2)}) copy-start(bf16[256,1024]{1,0:T(8,128)(2,1)} %param.32) | copy-start | bytes 1572868
  71.0 26.8 %all-reduce.5.cloned.1.call-start = ((), (), s32[]{:S(2)}) async-start(), calls=%async_computation.5 | async-start | bytes 524288 | tf_op jit(solution)/shard_map/psum | solution.py:137
  73.3 87.6 %reduce-scatter.2.cloned.1.call-start = ((), (), s32[]{:S(2)}) async-start(), calls=%async_computation.6 | async-start | bytes 1114112 | tf_op jit(solution)/shard_map/reduce_scatter | solution.py:143
  98.8 12.6 %copy-start.4 = (bf16[1,2048,256]{2,1,0:T(8,128)(2,1)S(1)}, bf16[1,2048,256]{2,1,0:T(8,128)(2,1)}, u32[]{:S(2)}) copy-start(bf16[1,2048,256]{2,1,0:T(8,128)(2,1)} %param.35) | copy-start | bytes 3145732
  114.8 19.0 %copy-start.11 = (bf16[2048]{0:T(1024)(128)(2,1)S(1)}, bf16[2048]{0:T(1024)(128)(2,1)}, u32[]{:S(2)}) copy-start(bf16[2048]{0:T(1024)(128)(2,1)} %param.29) | copy-start | bytes 12292
  114.8 19.0 %copy-start.9 = (f32[16,6]{0,1:T(8,128)S(1)}, f32[16,6]{0,1:T(8,128)}, u32[]{:S(2)}) copy-start(f32[16,6]{0,1:T(8,128)} %param.34) | copy-start | bytes 1156
  126.9 34.0 %copy-start.6 = (f32[16,2048]{1,0:T(8,128)S(1)}, f32[16,2048]{1,0:T(8,128)}, u32[]{:S(2)}) copy-start(f32[16,2048]{1,0:T(8,128)} %get-tuple-element.6) | copy-start | bytes 393220
  128.2 20.7 %all-to-all-start.2 = ((bf16[16,12,1024]{2,1,0:T(8,128)(2,1)}), bf16[16,12,1024]{2,1,0:T(8,128)(2,1)S(1)}, u32[]{:S(2)}, u32[]{:S(2)}) async-start(bf16[16,12,1024]{2,1,0:T(8,128)(2,1)} %copy.64), calls=%async_computation.2 | async-start | bytes 1048576 | tf_op jit(solution)/shard_map/all_to_all | solution.py:124
Sparse Core Ops, SparseCore 0:
  17.0 23.6 all-reduce.2
  74.0 23.6 all-reduce.4
  101.4 59.4 reduce-scatter.1
where the time goes:
time: 170 us; the launch traced here: 169 us
  waiting for transfers between devices  74.1 us (44%)
  blocking collectives  46 us (27%)
  matrix products  16.6 us (10%)
  between operations  13.5 us (8%)
  starting transfers between devices  9.31 us (5%)
  other arithmetic  6.78 us (4%)
  local copies, waits for them, and re-layouts  2.79 us (2%)
    psum x1, waiting for transfers between devices, on_device(): lax.psum(pre_parts.astype(jnp.float32).astype(jnp.bfloat16), 'tp')  24.4 us
    psum x1, waiting for transfers between devices, on_device(): lax.psum(head_partial.astype(jnp.float32).astype(jnp.bfloat16), 'tp')  23 us
    all_gather x1, blocking collectives, on_device(): lax.all_gather(own_cols, 'ep', axis=0, tiled=True)  22.9 us
    all_to_all x1, waiting for transfers between devices, on_device(): lax.all_to_all(mine, 'ep', split_axis=0, concat_axis=0, tiled=True)  14.8 us
    all_to_all x1, blocking collectives, on_device(): lax.all_to_all(blocks_out, 'tp', split_axis=3, concat_axis=3, tiled=True)  12.1 us
    reduce_scatter x1, waiting for transfers between devices, on_device(): lax.psum_scatter(jnp.dot(dense_hidden, dense_down, preferred_element_type...  11.9 us
    all_gather x1, blocking collectives, on_device(): received = lax.all_gather(received, 'tp', axis=2, tiled=True)  11 us
    all_to_all x1, starting transfers between devices, on_device(): lax.all_to_all(mine, 'ep', split_axis=0, concat_axis=0, tiled=True)  5.62 us
  transfers between devices with their start and end apart: 5, of which 4 were waited for; matrix products, arithmetic and copies ran while one was open for 6% of the time, Pallas kernels for 0%

commit v1 on v0

--- a/solution.py
+++ b/solution.py
@@ -134,9 +134,9 @@
         both_weights,
         preferred_element_type=jnp.float32,
     ).astype(jnp.bfloat16)
-    pre_total = lax.psum(pre_parts.astype(jnp.float32).astype(jnp.bfloat16), "tp").astype(
-        jnp.float32
-    )
+    pre_total = jnp.sum(
+        lax.all_gather(pre_parts.astype(jnp.float32).astype(jnp.bfloat16), axis_name="tp"), axis=0
+    ).astype(jnp.float32)
     dense_hidden = (jax.nn.silu(pre_total[:, :hidden_units]) * pre_total[:, hidden_units:]).astype(
         jnp.bfloat16
     )

time: 170 us -> 157 us (0.924)
  waiting for transfers between devices: 74.1 us -> 48.4 us
  blocking collectives: 46 us -> 59.7 us
    psum x1 -> x0, waiting for transfers between devices: 24.4 us -> none  [on_device(): lax.psum(pre_parts.astype(jnp.float32).astype(jnp.bfloat16), 'tp')]
    all_gather x0 -> x1, blocking collectives: none -> 9.22 us  [on_device(): lax.all_gather(pre_parts.astype(jnp.float32).astype(jnp.bfloat16), axis_n...]
    all_gather x1, blocking collectives: 22.9 us -> 26.9 us  [on_device(): lax.all_gather(own_cols, 'ep', axis=0, tiled=True)]
    all_to_all x1, starting transfers between devices: 3.57 us -> 5.62 us  [on_device(): lax.all_to_all(packed, 'ep', split_axis=0, concat_axis=0, tiled=True)]
    all_to_all x1, starting transfers between devices: 5.62 us -> 3.57 us  [on_device(): lax.all_to_all(mine, 'ep', split_axis=0, concat_axis=0, tiled=True)]
  transfers between devices with their start and end apart: 5 -> 4, of which waited for: 4 -> 3; matrix products, arithmetic and copies ran while one was open for 6% -> 6% of each run, Pallas kernels for 0% -> 0%
where the time goes in v1:
time: 157 us; the launch traced here: 156 us
  blocking collectives  59.7 us (38%)
  waiting for transfers between devices  48.4 us (31%)
  matrix products  16.1 us (10%)
  between operations  13.8 us (9%)
  starting transfers between devices  9.27 us (6%)
  other arithmetic  5.93 us (4%)
  local copies, waits for them, and re-layouts  2.79 us (2%)
    all_gather x1, blocking collectives, on_device(): lax.all_gather(own_cols, 'ep', axis=0, tiled=True)  26.9 us
    psum x1, waiting for transfers between devices, on_device(): lax.psum(head_partial.astype(jnp.float32).astype(jnp.bfloat16), 'tp')  23 us
    all_to_all x1, waiting for transfers between devices, on_device(): lax.all_to_all(mine, 'ep', split_axis=0, concat_axis=0, tiled=True)  14.3 us
    all_to_all x1, blocking collectives, on_device(): lax.all_to_all(blocks_out, 'tp', split_axis=3, concat_axis=3, tiled=True)  12.4 us
    all_gather x1, blocking collectives, on_device(): received = lax.all_gather(received, 'tp', axis=2, tiled=True)  11.2 us
    reduce_scatter x1, waiting for transfers between devices, on_device(): lax.psum_scatter(jnp.dot(dense_hidden, dense_down, preferred_element_type...  11.1 us
    all_gather x1, blocking collectives, on_device(): lax.all_gather(pre_parts.astype(jnp.float32).astype(jnp.bfloat16), axis_n...  9.22 us
    all_to_all x1, starting transfers between devices, on_device(): lax.all_to_all(packed, 'ep', split_axis=0, concat_axis=0, tiled=True)  5.62 us
  transfers between devices with their start and end apart: 4, of which 3 were waited for; matrix products, arithmetic and copies ran while one was open for 6% of the time, Pallas kernels for 0%

profile of v1, /device:TPU:0, one launch (start us, length us, event | category | flops | bytes accessed | tf_op | source)
XLA Modules:
  0.0 155.9 jit_solution(6780330245404084669)
XLA Ops:
  6.5 0.0 copy-start
  6.5 0.0 all-reduce.2.cloned.1.call-start
  6.6 0.8 convert_element_type.79
  7.4 1.0 fusion.30
  8.5 1.6 %fusion.47 = f32[16,256]{1,0:T(8,128)S(1)} fusion(bf16[2048,256]{1,0:T(8,128)(2,1)} %param.25, bf16[16,2048]{1,0:T(8,128)(2,1)} %param.20, f32[2048]{0:T(1024)} %param.23, f32[16]{0:T(128)S(1)} %add_rsqrt_fusion.2), kind=kOutput, calls=%fused_computation.81 | convolution fusion | flops 16908288 | bytes 1138752 | tf_op jit(solution)/shard_map/dot_general | solution.py:59
  10.1 1.6 %fusion.45 = f32[16,256]{1,0:T(8,128)S(1)} fusion(bf16[2048,256]{1,0:T(8,128)(2,1)} %param.26, bf16[16,2048]{1,0:T(8,128)(2,1)} %param.20, f32[2048]{0:T(1024)} %param.23, f32[16]{0:T(128)S(1)} %add_rsqrt_fusion.2), kind=kOutput, calls=%fused_computation.80 | convolution fusion | flops 16908288 | bytes 1138752 | tf_op jit(solution)/shard_map/dot_general | solution.py:62
  11.6 0.0 copy-done.1
  11.7 0.0 copy-done.7
  11.7 1.5 fusion.49
  13.2 0.0 copy-start.3
  13.2 0.1 fusion.41
  13.3 0.1 multiply_cosine_fusion
  13.4 0.0 copy-start.10
  13.4 0.1 multiply_subtract_fusion
  13.5 0.1 pad_maximum_fusion
  13.6 0.0 copy-done.2
  13.7 2.1 %fusion = f32[16,2,1,128]{3,2,1,0:T(1,128)S(1)} fusion(f32[16,2,128,1]{2,3,1,0:T(1,128)S(1)} %bitcast.88, f32[16,2,128,128]{3,2,1,0:T(8,128)S(1)} %copy-done.2, f32[16,2,128]{2,1,0:T(2,128)S(1)} %mul.244, f32[16,2,128]{2,1,0:T(2,128)S(1)} %get-tuple-element.17, f32[2]{0:T(128)S(1)} %power_subtract_fusion), kind=kOutput, calls=%fused_computation.2 | convolution fusion | flops 7864320 | bytes 2162696 | tf_op jit(solution)/shard_map/bhd,bhde->bhe/dot_general | solution.py:75
  15.7 0.1 multiply_reduce_fusion.1
  15.8 0.1 multiply_convert_fusion.1
  15.9 0.0 copy-done.3
  15.9 0.9 convolution_convert_fusion.1
  16.8 0.0 all-reduce.2.cloned.1.call-update
  16.9 0.1 copy.59
  16.9 0.1 eq.30
  17.0 0.1 fusion.38
  17.1 0.1 reduce_window_sum.11
  17.3 0.2 select_reduce_fusion.1
  17.4 0.1 reshape.154
  17.5 0.1 copy.60
  17.6 0.1 fusion.37
  17.7 23.0 %all-reduce.2.cloned.1.call-done = bf16[16,2048]{1,0:T(8,128)(2,1)} async-done(((bf16[16,2048]{1,0:T(8,128)(2,1)}), bf16[16,2048]{1,0:T(8,128)(2,1)}) %all-reduce.2.cloned.1.call-update) | async-done | bytes 65552 | tf_op jit(solution)/shard_map/psum | solution.py:81
  40.7 1.6 %convert_add_fusion = (f32[16,2048]{1,0:T(8,128)}, f32[16]{0:T(128)S(1)}) fusion(bf16[16,2048]{1,0:T(8,128)(2,1)S(1)} %copy-done.1, bf16[16,2048]{1,0:T(8,128)(2,1)} %all-reduce.2.cloned.1.call-done), kind=kLoop, calls=%fused_computation.38 | loop fusion | flops 163824 | bytes 262208 | tf_op jit(solution)/shard_map/add | solution.py:84
  42.3 0.9 multiply_convert_fusion
  43.3 0.3 convolution_convert_fusion.2
  43.6 0.9 reshape.155
  44.5 5.6 %all-to-all-start = ((bf16[16,12,1024]{2,1,0:T(8,128)(2,1)}), bf16[16,12,1024]{2,1,0:T(8,128)(2,1)S(1)}, u32[]{:S(2)}, u32[]{:S(2)}) async-start(bf16[16,12,1024]{2,1,0:T(8,128)(2,1)} %reshape.155), calls=%async_computation | async-start | bytes 1048576 | tf_op jit(solution)/shard_map/all_to_all | solution.py:106
  50.1 0.0 reduce-scatter.2.cloned.1.call-start
  50.1 26.9 %all_gather.13 = bf16[256,1024]{1,0:T(8,128)(2,1)S(1)} all-gather(bf16[16,1024]{1,0:T(8,128)(2,1)S(1)} %constant_dynamic-slice_fusion), channel_id=1, replica_groups=mesh['ep'=16,'tp'=2] {'ep'}, dimensions={0}, use_global_device_ids=true | all-gather | bytes 557056 | tf_op jit(solution)/shard_map/all_gather | solution.py:133
  77.0 1.7 %convolution_convert_fusion.3 = bf16[256,512]{1,0:T(8,128)(2,1)S(1)} fusion(bf16[256,1024]{1,0:T(8,128)(2,1)S(1)} %all_gather.13, bf16[1024,256]{1,0:T(8,128)(2,1)} %param.31, bf16[1024,256]{1,0:T(8,128)(2,1)} %param.30), kind=kOutput, calls=%fused_computation.7 | convolution fusion | flops 270663680 | bytes 1835008 | tf_op jit(solution)/shard_map/dot_general | solution.py:132
  78.7 9.2 %all-gather = bf16[512,512]{1,0:T(8,128)(2,1)S(1)} all-gather(bf16[256,512]{1,0:T(8,128)(2,1)S(1)} %convolution_convert_fusion.3), channel_id=2, replica_groups=mesh['ep'=16,'tp'=2] {'tp'}, dimensions={0}, use_global_device_ids=true | all-gather | bytes 786432 | tf_op jit(solution)/shard_map/all_gather | solution.py:138
  87.9 0.1 reduce_sum.85
  88.0 0.1 convert_element_type.94
  88.1 0.0 copy-start.4
  88.1 1.3 fusion.33
  89.4 0.0 reduce-scatter.2.cloned.1.call-update
  89.4 0.0 all-to-all-done
  89.5 0.2 copy.61
  89.7 11.2 %all_gather.12 = bf16[16,12,2048]{2,0,1:T(8,128)(2,1)S(1)} all-gather(bf16[16,12,1024]{2,0,1:T(8,128)(2,1)S(1)} %copy.61), channel_id=1, replica_groups=mesh['ep'=16,'tp'=2] {'tp'}, dimensions={2}, use_global_device_ids=true | all-gather | bytes 1179648 | tf_op jit(solution)/shard_map/all_gather | solution.py:107
  100.9 0.0 copy-done.4
  100.9 1.1 convolution_bitcast_fusion.1
  101.9 2.3 %convolution_convert_fusion = bf16[16,12,2048]{2,0,1:T(8,128)(2,1)S(1)} fusion(bf16[1,256,2048]{2,1,0:T(8,128)(2,1)S(1)} %copy-done, bf16[16,12,2048]{2,0,1:T(8,128)(2,1)S(1)} %all_gather.12, bf16[1,2048,256]{2,1,0:T(8,128)(2,1)} %param.36, f32[16,1,12,256]{3,0,2,1:T(8,128)} %convolution_bitcast_fusion.1), kind=kOutput, calls=%fused_computation | convolution fusion | flops 403341312 | bytes 3866624 | tf_op jit(solution)/shard_map/skcw,kwd->skcd/dot_general | solution.py:115
  104.2 0.1 copy.77
  104.3 0.0 copy-start.11
  104.3 0.0 copy-start.9
  104.3 12.4 %all_to_all.15 = bf16[16,1,12,2,1024]{4,0,2,1,3:T(8,128)(2,1)S(1)} all-to-all(bf16[16,1,12,2,1024]{4,0,2,1,3:T(8,128)(2,1)S(1)} %bitcast.83), channel_id=1, replica_groups=mesh['ep'=16,'tp'=2] {'tp'}, dimensions={3} | all-to-all | bytes 1572864 | tf_op jit(solution)/shard_map/all_to_all | solution.py:121
  116.7 0.2 reduce_sum.84
  116.9 1.0 copy.64
  118.0 3.6 %all-to-all-start.2 = ((bf16[16,12,1024]{2,1,0:T(8,128)(2,1)}), bf16[16,12,1024]{2,1,0:T(8,128)(2,1)S(1)}, u32[]{:S(2)}, u32[]{:S(2)}) async-start(bf16[16,12,1024]{2,1,0:T(8,128)(2,1)} %copy.64), calls=%async_computation.2 | async-start | bytes 1048576 | tf_op jit(solution)/shard_map/all_to_all | solution.py:124
  121.6 0.1 select_reduce_fusion
  121.7 0.1 fusion.12
  121.8 14.3 %all-to-all-done.2 = bf16[16,12,1024]{2,1,0:T(8,128)(2,1)S(1)} async-done(((bf16[16,12,1024]{2,1,0:T(8,128)(2,1)}), bf16[16,12,1024]{2,1,0:T(8,128)(2,1)S(1)}, u32[]{:S(2)}, u32[]{:S(2)}) %all-to-all-start.2) | async-done | bytes 393248 | tf_op jit(solution)/shard_map/all_to_all | solution.py:124
  136.1 0.1 reshape.161
  136.2 11.1 %reduce-scatter.2.cloned.1.call-done = f32[16,1024]{1,0:T(8,128)} async-done(((f32[256,1024]{1,0:T(8,128)}), f32[16,1024]{1,0:T(8,128)}) %reduce-scatter.2.cloned.1.call-update) | async-done | bytes 65552 | tf_op jit(solution)/shard_map/reduce_scatter | solution.py:143
  147.3 1.7 %fusion.8 = bf16[16,1024]{1,0:T(8,128)(2,1)} fusion(f32[192,16]{0,1:T(8,128)S(1)} %select_reduce_fusion, bf16[192,1024]{1,0:T(8,128)(2,1)S(1)} %reshape.161, f32[16,1024]{1,0:T(8,128)} %reduce-scatter.2.cloned.1.call-done, f32[16,2048]{1,0:T(8,128)S(1)} %copy-done.6, s32[]{:T(128)S(6)} %select_n.8, f32[16]{0:T(128)S(1)} %fusion.12), kind=kOutput, calls=%fused_computation.15 | convolution fusion | flops 37814272 | bytes 569412 | tf_op jit(solution)/shard_map/dot_general | solution.py:125
  (26 shorter events, 0.2 us)
Async XLA Ops:
  6.5 95.4 %copy-start = (bf16[1,256,2048]{2,1,0:T(8,128)(2,1)S(1)}, bf16[1,256,2048]{2,1,0:T(8,128)(2,1)}, u32[]{:S(2)}) copy-start(bf16[1,256,2048]{2,1,0:T(8,128)(2,1)} %param.37) | copy-start | bytes 3145732
  6.5 5.1 %copy-start.1 = (bf16[16,2048]{1,0:T(8,128)(2,1)S(1)}, bf16[16,2048]{1,0:T(8,128)(2,1)}, u32[]{:S(2)}) copy-start(bf16[16,2048]{1,0:T(8,128)(2,1)} %param.20) | copy-start | bytes 196612
  6.5 5.1 %copy-start.7 = (f32[2048]{0:T(1024)S(1)}, f32[2048]{0:T(1024)}, u32[]{:S(2)}) copy-start(f32[2048]{0:T(1024)} %param.23) | copy-start | bytes 24580
  6.5 7.1 %copy-start.2 = (f32[16,2,128,128]{3,2,1,0:T(8,128)S(1)}, f32[16,2,128,128]{3,2,1,0:T(8,128)}, u32[]{:S(2)}) copy-start(f32[16,2,128,128]{3,2,1,0:T(8,128)} %param.22) | copy-start | bytes 6291460
  6.5 34.1 %all-reduce.2.cloned.1.call-start = ((), (), s32[]{:S(2)}) async-start(), calls=%async_computation.4 | async-start | bytes 131072 | tf_op jit(solution)/shard_map/psum | solution.py:81
  13.2 3.7 %copy-start.8 = (s32[16,6]{0,1:T(8,128)S(1)}, s32[16,6]{0,1:T(8,128)}, u32[]{:S(2)}) copy-start(s32[16,6]{0,1:T(8,128)} %param.33) | copy-start | bytes 1156
  13.2 2.7 %copy-start.3 = (bf16[256,2048]{1,0:T(8,128)(2,1)S(1)}, bf16[256,2048]{1,0:T(8,128)(2,1)}, u32[]{:S(2)}) copy-start(bf16[256,2048]{1,0:T(8,128)(2,1)} %param.27) | copy-start | bytes 3145732
  13.4 28.9 %copy-start.10 = (f32[2048]{0:T(1024)S(1)}, f32[2048]{0:T(1024)}, u32[]{:S(2)}) copy-start(f32[2048]{0:T(1024)} %param.28) | copy-start | bytes 24580
  44.5 45.0 %all-to-all-start = ((bf16[16,12,1024]{2,1,0:T(8,128)(2,1)}), bf16[16,12,1024]{2,1,0:T(8,128)(2,1)S(1)}, u32[]{:S(2)}, u32[]{:S(2)}) async-start(bf16[16,12,1024]{2,1,0:T(8,128)(2,1)} %reshape.155), calls=%async_computation | async-start | bytes 1048576 | tf_op jit(solution)/shard_map/all_to_all | solution.py:106
  50.1 97.2 %reduce-scatter.2.cloned.1.call-start = ((), (), s32[]{:S(2)}) async-start(), calls=%async_computation.5 | async-start | bytes 1114112 | tf_op jit(solution)/shard_map/reduce_scatter | solution.py:143
  77.0 11.1 %copy-start.5 = (bf16[256,1024]{1,0:T(8,128)(2,1)S(1)}, bf16[256,1024]{1,0:T(8,128)(2,1)}, u32[]{:S(2)}) copy-start(bf16[256,1024]{1,0:T(8,128)(2,1)} %param.32) | copy-start | bytes 1572868
  88.1 12.8 %copy-start.4 = (bf16[1,2048,256]{2,1,0:T(8,128)(2,1)S(1)}, bf16[1,2048,256]{2,1,0:T(8,128)(2,1)}, u32[]{:S(2)}) copy-start(bf16[1,2048,256]{2,1,0:T(8,128)(2,1)} %param.35) | copy-start | bytes 3145732
  104.3 17.2 %copy-start.11 = (bf16[2048]{0:T(1024)(128)(2,1)S(1)}, bf16[2048]{0:T(1024)(128)(2,1)}, u32[]{:S(2)}) copy-start(bf16[2048]{0:T(1024)(128)(2,1)} %param.29) | copy-start | bytes 12292
  104.3 17.3 %copy-start.9 = (f32[16,6]{0,1:T(8,128)S(1)}, f32[16,6]{0,1:T(8,128)}, u32[]{:S(2)}) copy-start(f32[16,6]{0,1:T(8,128)} %param.34) | copy-start | bytes 1156
  116.7 30.6 %copy-start.6 = (f32[16,2048]{1,0:T(8,128)S(1)}, f32[16,2048]{1,0:T(8,128)}, u32[]{:S(2)}) copy-start(f32[16,2048]{1,0:T(8,128)} %get-tuple-element.6) | copy-start | bytes 393220
  118.0 18.2 %all-to-all-start.2 = ((bf16[16,12,1024]{2,1,0:T(8,128)(2,1)}), bf16[16,12,1024]{2,1,0:T(8,128)(2,1)S(1)}, u32[]{:S(2)}, u32[]{:S(2)}) async-start(bf16[16,12,1024]{2,1,0:T(8,128)(2,1)} %copy.64), calls=%async_computation.2 | async-start | bytes 1048576 | tf_op jit(solution)/shard_map/all_to_all | solution.py:124
Sparse Core Ops, SparseCore 0:
  17.0 23.6 all-reduce.1
  89.6 57.7 reduce-scatter.1
